TPU v7x, 32 devices: a whole 2x2x4 slice. The times are simulated.
32 devices in a mesh: sp: 8 (over z, x), tp: 4 (over y, core).
Axes of the slice: x: 2, y: 2, z: 4, core: 2. Of those that a mesh axis runs over, the one named last changes fastest.
Arguments:
- latents: bfloat16 [4096, 2048], P(('sp', 'tp')), may hold values from -6 to 6
- context: bfloat16 [512, 2048], P('sp'), may hold values from -6 to 6
- cond: float32 [2048], P('sp'), may hold values from -6 to 6
- ctx_cond: float32 [2048], P('sp'), may hold values from -6 to 6
- mod_weight: float32 [2048, 6144], P('sp', 'tp'), may hold values from -0.125 to 0.125
- query_weight: bfloat16 [2048, 2048], P(None, 'tp'), may hold values from -1 to 1, as said below
- key_matrix: bfloat16 [2048, 1024], P(None, 'tp'), may hold values from -1 to 1, as said below
- value_matrix: bfloat16 [2048, 1024], P(None, 'tp'), may hold values from -0.125 to 0.125
- out_weight: bfloat16 [2048, 2048], P('tp'), may hold values from -0.125 to 0.125
- query_gain: float32 [128], replicated, may hold values from 0.7 to 7
- key_gain: float32 [128], replicated, may hold values from 0.7 to 7
Outputs:
- updated: bfloat16 [4096, 2048], P(('sp', 'tp'))
Inputs may be any that keep to these rules, and one draw needn't show every extreme that they name: `query_weight`: entries of order 2048 to the power -1/2. `key_matrix`: entries of order 2048 to the power -1/2.
All inputs are finite; a program needn't handle non-finite values.
Results may differ from a plain program's by a relative error of at most 0.0085.
The roundings to bfloat16 on the way count: a program that leaves them out, or rounds other values in their place, can miss the bound.
Values may be sent and summed in bfloat16 or wider, within the bound.
A program may use at most 128 MiB of HBM per device.

v0:
```python
import math
import jax
import jax.numpy as jnp
from jax import lax
from jax.sharding import PartitionSpec as P

GRID_W = 64
NORM_EPS = 1e-06
ROPE_BASE = 10000.0


def normalize(latent_value_rows):
    return latent_value_rows * lax.rsqrt(
        jnp.mean(latent_value_rows * latent_value_rows, axis=-1, keepdims=True) + NORM_EPS
    )


def rotate(latent_value_rows, positions):
    quarter = latent_value_rows.shape[-1] // 2
    inv_freq = ROPE_BASE ** (-jnp.arange(quarter, dtype=jnp.float32) / quarter)
    angles = positions.astype(jnp.float32)[:, None] * inv_freq[None, :]
    cos_table = jnp.cos(angles)[:, None, :]
    sin_table = jnp.sin(angles)[:, None, :]
    first, second = (latent_value_rows[..., :quarter], latent_value_rows[..., quarter:])
    return jnp.concatenate(
        [first * cos_table - second * sin_table, second * cos_table + first * sin_table], axis=-1
    )


def axial(latent_value_rows, positions):
    half_dim = latent_value_rows.shape[-1] // 2
    return jnp.concatenate(
        [
            rotate(latent_value_rows[..., :half_dim], positions // GRID_W),
            rotate(latent_value_rows[..., half_dim:], positions % GRID_W),
        ],
        axis=-1,
    )


def modulate(latent_value_rows, mod_row):
    model_width = latent_value_rows.shape[-1]
    shift_vec = mod_row[:model_width]
    scale_vec = mod_row[model_width : 2 * model_width]
    return (
        normalize(latent_value_rows.astype(jnp.float32)) * (1.0 + scale_vec) + shift_vec
    ).astype(jnp.bfloat16)


def body(
    latents,
    context,
    cond,
    ctx_cond,
    mod_weight,
    query_weight,
    key_matrix,
    value_matrix,
    out_weight,
    query_gain,
    key_gain,
):
    model_width = latents.shape[1]
    head_dim = query_gain.shape[0]
    sp_count = lax.axis_size("sp")
    partials = jnp.dot(
        jax.nn.silu(jnp.stack([cond, ctx_cond])), mod_weight, precision=lax.Precision.HIGHEST
    )
    summed = lax.psum(partials, "sp")
    modulation = lax.all_gather(summed, "tp", axis=1, tiled=True)
    gate_vec = modulation[0, 2 * model_width :]
    normalised_rows = modulate(latents, modulation[0])
    prefix_normalised = modulate(context, modulation[1])
    query_cols = query_weight.shape[1]
    key_cols = key_matrix.shape[1]
    piece = lax.all_gather(normalised_rows, "tp", axis=0, tiled=True)
    projected = jnp.concatenate(
        [
            jnp.dot(piece, query_weight, preferred_element_type=jnp.float32),
            jnp.dot(piece, key_matrix, preferred_element_type=jnp.float32),
            jnp.dot(piece, value_matrix, preferred_element_type=jnp.float32),
        ],
        axis=1,
    )
    row_count = projected.shape[0]
    positions = lax.axis_index("sp") * row_count + jnp.arange(row_count, dtype=jnp.int32)
    query_heads = projected[:, :query_cols].reshape(row_count, -1, head_dim)
    query_heads = axial(normalize(query_heads) * query_gain, positions).astype(jnp.bfloat16)
    key_heads = projected[:, query_cols : query_cols + key_cols].reshape(row_count, -1, head_dim)
    key_heads = axial(normalize(key_heads) * key_gain, positions).astype(jnp.bfloat16)
    value_heads = (
        projected[:, query_cols + key_cols :].reshape(row_count, -1, head_dim).astype(jnp.bfloat16)
    )
    key_part = jnp.dot(prefix_normalised, key_matrix, preferred_element_type=jnp.float32).reshape(
        prefix_normalised.shape[0], -1, head_dim
    )
    value_part = jnp.dot(
        prefix_normalised, value_matrix, preferred_element_type=jnp.float32
    ).reshape(prefix_normalised.shape[0], -1, head_dim)
    local_keys = (normalize(key_part) * key_gain).astype(jnp.bfloat16)
    local_values = value_part.astype(jnp.bfloat16)
    prefix_keys, prefix_values = (
        lax.all_gather(local_keys, "sp", axis=0, tiled=True),
        lax.all_gather(local_values, "sp", axis=0, tiled=True),
    )
    kv_local = key_heads.shape[1]
    group_size = query_heads.shape[1] // kv_local
    grouped = query_heads.reshape(row_count, kv_local, group_size, head_dim).transpose(1, 2, 0, 3)
    grouped = grouped.reshape(kv_local, group_size * row_count, head_dim)
    inv_root = head_dim ** (-0.5)
    lift = math.log(sp_count * row_count / (2.0 * prefix_keys.shape[0]))
    ctx_scores = (
        jnp.einsum("hqd,khd->hqk", grouped, prefix_keys, preferred_element_type=jnp.float32)
        * inv_root
        + lift
    )
    top_init = jnp.max(ctx_scores, axis=-1)
    ctx_weights = jnp.exp(ctx_scores - top_init[..., None])
    initial = (
        top_init,
        jnp.sum(ctx_weights, axis=-1),
        jnp.einsum(
            "hqk,khd->hqd",
            ctx_weights.astype(jnp.bfloat16),
            prefix_values,
            preferred_element_type=jnp.float32,
        ),
    )

    def update(state_now, key_block, value_block):
        top_old, total_old, acc_old = state_now
        scores = (
            jnp.einsum("hqd,khd->hqk", grouped, key_block, preferred_element_type=jnp.float32)
            * inv_root
        )
        top_new = jnp.maximum(top_old, jnp.max(scores, axis=-1))
        factor = jnp.exp(top_old - top_new)
        weights_now = jnp.exp(scores - top_new[..., None])
        acc_new = acc_old * factor[..., None] + jnp.einsum(
            "hqk,khd->hqd",
            weights_now.astype(jnp.bfloat16),
            value_block,
            preferred_element_type=jnp.float32,
        )
        return (top_new, total_old * factor + jnp.sum(weights_now, axis=-1), acc_new)

    key_piece = lax.all_gather(key_heads, "sp", axis=0, tiled=True)
    value_piece = lax.all_gather(value_heads, "sp", axis=0, tiled=True)
    key_count = key_piece.shape[0]
    rows_per_block = math.gcd(key_count, 2048)
    block_count = key_count // rows_per_block
    key_blocks = key_piece.reshape(block_count, rows_per_block, kv_local, head_dim)
    value_blocks = value_piece.reshape(block_count, rows_per_block, kv_local, head_dim)

    def one_step(state_in, blocks_in):
        return (update(state_in, blocks_in[0], blocks_in[1]), None)

    state_out, _ = lax.scan(one_step, initial, (key_blocks, value_blocks))
    top_fin, total_fin, acc_fin = state_out
    attended = (acc_fin / total_fin[..., None]).astype(jnp.bfloat16)
    attended = (
        attended.reshape(kv_local, group_size, row_count, head_dim)
        .transpose(2, 0, 1, 3)
        .reshape(row_count, -1)
    )
    mixed_rows = lax.psum_scatter(
        jnp.dot(attended, out_weight, preferred_element_type=jnp.float32).astype(jnp.bfloat16),
        "tp",
        scatter_dimension=0,
        tiled=True,
    ).astype(jnp.float32)
    return (latents.astype(jnp.float32) + gate_vec * normalize(mixed_rows)).astype(jnp.bfloat16)


def solution(mesh):
    placed = (
        P(("sp", "tp"), None),
        P("sp", None),
        P("sp"),
        P("sp"),
        P("sp", "tp"),
        P(None, "tp"),
        P(None, "tp"),
        P(None, "tp"),
        P("tp", None),
        P(),
        P(),
    )
    return jax.shard_map(
        body, mesh=mesh, in_specs=placed, out_specs=P(("sp", "tp"), None), check_vma=False
    )
```

profile of v0, /device:TPU:0, one launch (start us, length us, event | category | flops | bytes accessed | tf_op | source)
XLA Modules:
  0.0 286.1 jit_solution(9915169423210026204)
XLA Ops:
  6.5 2.4 fusion.41
  9.0 38.8 %psum.7 = f32[2,1536]{1,0:T(2,128)S(1)} all-reduce(f32[2,1536]{1,0:T(2,128)S(1)} %fusion.41), channel_id=1, replica_groups=mesh['sp'=8,'tp'=4] {'sp'}, use_global_device_ids=true, to_apply=%region_0.1 | all-reduce | flops 3072 | bytes 24576 | tf_op jit(solution)/shard_map/psum | solution.py:69
  47.8 5.2 %all_gather.18 = f32[2,6144]{1,0:T(2,128)S(1)} all-gather(f32[2,1536]{1,0:T(2,128)S(1)} %psum.7), channel_id=1, replica_groups=mesh['sp'=8,'tp'=4] {'tp'}, dimensions={1}, use_global_device_ids=true | all-gather | bytes 61440 | tf_op jit(solution)/shard_map/all_gather | solution.py:70
  53.6 1.2 fusion.27
  54.9 2.1 fusion.30
  59.6 17.4 %all-gather.4.cloned.1.call-done = bf16[512,2048]{1,0:T(8,128)(2,1)} async-done(((bf16[128,2048]{1,0:T(8,128)(2,1)}), bf16[512,2048]{1,0:T(8,128)(2,1)}) %all-gather.4.cloned.1.call-update) | async-done | bytes 2097168 | tf_op jit(solution)/shard_map/all_gather | solution.py:76
  77.0 4.0 %multiply_reduce_fusion.1 = (f32[512,2]{0,1:T(2,128)}, f32[512,256]{0,1:T(8,128)}) fusion(bf16[512,2048]{1,0:T(8,128)(2,1)} %all-gather.4.cloned.1.call-done, bf16[2048,256]{1,0:T(8,128)(2,1)} %param.19), kind=kOutput, calls=%fused_computation.57 | convolution fusion | flops 537132032 | bytes 3674112 | tf_op jit(solution)/shard_map/dot_general | solution.py:80
  81.0 1.3 copy.80
  83.8 1.5 subtract_convert_fusion.1
  87.3 3.3 %convolution_convert_fusion.1 = bf16[512,256]{0,1:T(8,128)(2,1)} fusion(bf16[512,2048]{1,0:T(8,128)(2,1)} %all-gather.4.cloned.1.call-done, bf16[2048,256]{1,0:T(8,128)(2,1)} %param.20), kind=kOutput, calls=%fused_computation.32 | convolution fusion | flops 537001984 | bytes 3407872 | tf_op jit(solution)/shard_map/dot_general | solution.py:81
  90.6 1.8 copy.85
  95.8 1.6 fusion.24
  98.4 31.6 %all_gather.20 = bf16[512,2,128]{2,0,1:T(8,128)(2,1)S(1)} all-gather(bf16[64,2,128]{2,0,1:T(8,128)(2,1)S(1)} %fusion.37), channel_id=1, replica_groups=mesh['sp'=8,'tp'=4] {'sp'}, dimensions={0}, use_global_device_ids=true | all-gather | bytes 294912 | tf_op jit(solution)/shard_map/all_gather | solution.py:103
  129.9 33.5 %all_gather.21 = bf16[512,2,128]{2,0,1:T(8,128)(2,1)} all-gather(bf16[64,2,128]{2,0,1:T(8,128)(2,1)S(1)} %bitcast.103), channel_id=1, replica_groups=mesh['sp'=8,'tp'=4] {'sp'}, dimensions={0}, use_global_device_ids=true | all-gather | bytes 294912 | tf_op jit(solution)/shard_map/all_gather | solution.py:104
  163.5 3.6 %multiply_reduce_fusion = (f32[512,4]{0,1:T(4,128)S(1)}, f32[512,512]{0,1:T(8,128)S(1)}) fusion(bf16[512,2048]{1,0:T(8,128)(2,1)} %all-gather.4.cloned.1.call-done, bf16[2048,512]{1,0:T(8,128)(2,1)} %param.18), kind=kOutput, calls=%fused_computation.44 | convolution fusion | flops 1074264064 | bytes 5251072 | tf_op jit(solution)/shard_map/dot_general | solution.py:79
  169.6 1.9 copy.74
  171.5 1.9 copy.75
  173.5 1.9 pad_maximum_fusion
  177.7 1.2 fusion.19
  179.0 10.1 %all-gather.8.cloned.1.call-done = bf16[4096,2,128]{2,0,1:T(8,128)(2,1)} async-done(((bf16[512,2,128]{2,0,1:T(8,128)(2,1)}), bf16[4096,2,128]{2,0,1:T(8,128)(2,1)}) %all-gather.8.cloned.1.call-update) | async-done | bytes 2097168 | tf_op jit(solution)/shard_map/all_gather | solution.py:148
  189.1 52.1 %while.14 = (s32[]{:T(128)}, f32[2,1024]{1,0:T(2,128)S(1)}, f32[2,1024]{1,0:T(2,128)S(1)}, f32[2,1024,128]{2,1,0:T(8,128)S(1)}, bf16[2,2048,2,128]{3,1,0,2:T(8,1...) while((s32[]{:T(128)}, f32[2,1024]{1,0:T(2,128)S(1)}, ...), condition=%wide.region_11.12_spmd, body=%wide.region_8.11_spmd.sunk | while | flops 2181566464 | bytes 55182420 | solution.py:158
  189.1 9.4 %bitcast_reduce_fusion.2 = (f32[2,1024]{1,0:T(2,128)S(1)}, f32[2,2048,1024]{2,1,0:T(8,128)}) fusion(bf16[2,1024,128]{2,1,0:T(8,128)(2,1)} %get-tuple-element.194, bf16[2,2048,2,128]{3,1,0,2:T(8,128)(2,1)} %get-tuple-element.193, s32[]{:T(128)} %get-tuple-element.181), kind=kOutput, calls=%fused_computation.1.clone.1 | convolution fusion | flops 1082128384 | bytes 18358784 | tf_op jit(solution)/shard_map/while/body/eval_jaxpr/hqd,khd->hqk/dot_general | solution.py:133
  198.5 8.5 %fusion.80 = f32[2,1024]{1,0:T(2,128)S(1)} fusion(f32[2,2048,1024]{2,1,0:T(8,128)} %get-tuple-element.170, f32[2,1024]{1,0:T(2,128)S(1)} %max.4), kind=kLoop, calls=%fused_computation.4.clone.1 | loop fusion | flops 12580864 | bytes 16793600 | tf_op jit(solution)/shard_map/while/body/eval_jaxpr/reduce_sum | solution.py:145
  207.0 8.1 %fusion.81 = f32[2,1024,128]{2,1,0:T(8,128)S(1)} fusion(f32[2,2048,1024]{2,1,0:T(8,128)} %get-tuple-element.170, f32[2,1024]{1,0:T(2,128)S(1)} %max.4, bf16[2,2048,2,128]{3,1,0,2:T(8,128)(2,1)} %get-tuple-element.195, s32[]{:T(128)} %get-tuple-element.181, f32[2,1024,128]{2,1,0:T(8,128)S(1)} %get-tuple-element.184, f32[2,1024]{1,0:T(2,128)S(1)} %get-tuple-element.172), kind=kOutput, calls=%fused_computation.6.clone.1 | convolution fusion | flops 1086849024 | bytes 19939840 | tf_op jit(solution)/shard_map/while/body/eval_jaxpr/hqk,khd->hqd/dot_general | solution.py:139
  215.1 9.4 %bitcast_reduce_fusion.2 = (f32[2,1024]{1,0:T(2,128)S(1)}, f32[2,2048,1024]{2,1,0:T(8,128)}) fusion(bf16[2,1024,128]{2,1,0:T(8,128)(2,1)} %get-tuple-element.194, bf16[2,2048,2,128]{3,1,0,2:T(8,128)(2,1)} %get-tuple-element.193, s32[]{:T(128)} %get-tuple-element.181), kind=kOutput, calls=%fused_computation.1.clone.1 | convolution fusion | flops 1082128384 | bytes 18358784 | tf_op jit(solution)/shard_map/while/body/eval_jaxpr/hqd,khd->hqk/dot_general | solution.py:133
  224.5 8.5 %fusion.80 = f32[2,1024]{1,0:T(2,128)S(1)} fusion(f32[2,2048,1024]{2,1,0:T(8,128)} %get-tuple-element.170, f32[2,1024]{1,0:T(2,128)S(1)} %max.4), kind=kLoop, calls=%fused_computation.4.clone.1 | loop fusion | flops 12580864 | bytes 16793600 | tf_op jit(solution)/shard_map/while/body/eval_jaxpr/reduce_sum | solution.py:145
  233.1 8.1 %fusion.81 = f32[2,1024,128]{2,1,0:T(8,128)S(1)} fusion(f32[2,2048,1024]{2,1,0:T(8,128)} %get-tuple-element.170, f32[2,1024]{1,0:T(2,128)S(1)} %max.4, bf16[2,2048,2,128]{3,1,0,2:T(8,128)(2,1)} %get-tuple-element.195, s32[]{:T(128)} %get-tuple-element.181, f32[2,1024,128]{2,1,0:T(8,128)S(1)} %get-tuple-element.184, f32[2,1024]{1,0:T(2,128)S(1)} %get-tuple-element.172), kind=kOutput, calls=%fused_computation.6.clone.1 | convolution fusion | flops 1086849024 | bytes 19939840 | tf_op jit(solution)/shard_map/while/body/eval_jaxpr/hqk,khd->hqd/dot_general | solution.py:139
  242.3 1.2 copy.88
  243.6 2.6 convolution_convert_fusion
  246.3 29.9 %reduce-scatter.2.cloned.1.call-done = bf16[128,2048]{1,0:T(8,128)(2,1)} async-done(((bf16[512,2048]{1,0:T(8,128)(2,1)}), bf16[128,2048]{1,0:T(8,128)(2,1)}) %reduce-scatter.2.cloned.1.call-update) | async-done | bytes 524304 | tf_op jit(solution)/shard_map/reduce_scatter | solution.py:166
  276.2 1.2 fusion.25
  277.4 2.1 fusion.31
  (71 shorter events, 17.2 us)
Async XLA Ops:
  6.5 237.1 %copy-start = (bf16[512,2048]{1,0:T(8,128)(2,1)S(1)}, bf16[512,2048]{1,0:T(8,128)(2,1)}, u32[]{:S(2)}) copy-start(bf16[512,2048]{1,0:T(8,128)(2,1)} %param.21) | copy-start | bytes 6291460
  6.5 70.5 %all-gather.4.cloned.1.call-start = ((), (), s32[]{:S(2)}) async-start(), calls=%async_computation.1 | async-start | bytes 2621440 | tf_op jit(solution)/shard_map/all_gather | solution.py:76
  57.0 122.0 %all-gather.6.cloned.1.call-start = ((), (), s32[]{:S(2)}) async-start(), calls=%async_computation.2 | async-start | bytes 2359296 | tf_op jit(solution)/shard_map/all_gather | solution.py:147
  57.6 19.4 %copy-start.6 = (f32[512,32]{0,1:T(8,128)}, f32[512,32]{0,1:T(8,128)S(1)}, u32[]{:S(2)}) copy-start(f32[512,32]{0,1:T(8,128)S(1)} %get-tuple-element.112) | copy-start | bytes 196612
  57.6 19.4 %copy-start.8 = (f32[512,32]{0,1:T(8,128)}, f32[512,32]{0,1:T(8,128)S(1)}, u32[]{:S(2)}) copy-start(f32[512,32]{0,1:T(8,128)S(1)} %get-tuple-element.113) | copy-start | bytes 196612
  81.0 5.5 %copy-start.3 = (bf16[64,2048]{1,0:T(8,128)(2,1)S(1)}, bf16[64,2048]{1,0:T(8,128)(2,1)}, u32[]{:S(2)}) copy-start(bf16[64,2048]{1,0:T(8,128)(2,1)} %param.14) | copy-start | bytes 786436
  85.3 8.4 %copy-start.4 = (bf16[2048,256]{1,0:T(8,128)(2,1)S(1)}, bf16[2048,256]{1,0:T(8,128)(2,1)}, u32[]{:S(2)}) copy-start(bf16[2048,256]{1,0:T(8,128)(2,1)} %param.19) | copy-start | bytes 3145732
  86.5 102.6 %all-gather.8.cloned.1.call-start = ((), (), s32[]{:S(2)}) async-start(), calls=%async_computation.3 | async-start | bytes 2359296 | tf_op jit(solution)/shard_map/all_gather | solution.py:148
  92.4 183.8 %reduce-scatter.2.cloned.1.call-start = ((), (), s32[]{:S(2)}) async-start(), calls=%async_computation.4 | async-start | bytes 2621440 | tf_op jit(solution)/shard_map/reduce_scatter | solution.py:166
  93.1 0.6 copy-start.11
  163.4 3.6 %copy-start.12 = (f32[128]{0:T(128)S(1)}, f32[128]{0:T(128)}, u32[]{:S(2)}) copy-start(f32[128]{0:T(128)} %param.22) | copy-start | bytes 1540
  163.4 3.8 %copy-start.7 = (f32[512,32]{0,1:T(8,128)S(1)}, f32[512,32]{0,1:T(8,128)}, u32[]{:S(2)}) copy-start(f32[512,32]{0,1:T(8,128)} %copy-done.6) | copy-start | bytes 196612
  163.4 3.8 %copy-start.9 = (f32[512,32]{0,1:T(8,128)S(1)}, f32[512,32]{0,1:T(8,128)}, u32[]{:S(2)}) copy-start(f32[512,32]{0,1:T(8,128)} %copy-done.8) | copy-start | bytes 196612
  175.3 0.8 copy-start.1
  176.1 1.6 copy-start.5
  243.6 33.8 %copy-start.2 = (bf16[128,2048]{1,0:T(8,128)(2,1)S(1)}, bf16[128,2048]{1,0:T(8,128)(2,1)}, u32[]{:S(2)}) copy-start(bf16[128,2048]{1,0:T(8,128)(2,1)} %param.13) | copy-start | bytes 1572868
  243.6 33.8 %copy-start.10 = (f32[1,2048]{1,0:T(1,128)S(1)}, f32[1,2048]{1,0:T(1,128)}, u32[]{:S(2)}) copy-start(f32[1,2048]{1,0:T(1,128)} %get-tuple-element.103) | copy-start | bytes 24580
Sparse Core Ops, SparseCore 0:
  57.1 19.8 all-gather.3
  86.6 52.3 all-gather.5
  141.2 47.7 all-gather.7
  246.4 29.7 reduce-scatter.1
where the time goes:
time: 287 us; the launch traced here: 286 us
  blocking collectives  109 us (38%)
  waiting for transfers between devices  57.5 us (20%)
  matrix products  55.5 us (19%)
  other arithmetic  36.5 us (13%)
  local copies, waits for them, and re-layouts  13.9 us (5%)
  between operations  13.4 us (5%)
    psum x1, blocking collectives, body(): summed = lax.psum(partials, 'sp')  38.8 us
    all_gather x1, blocking collectives, body(): lax.all_gather(local_values, 'sp', axis=0, tiled=True)  33.5 us
    all_gather x1, blocking collectives, body(): lax.all_gather(local_keys, 'sp', axis=0, tiled=True)  31.6 us
    reduce_scatter x1, waiting for transfers between devices, body(): lax.psum_scatter(jnp.dot(attended, out_weight, preferred_element_type=jnp...  29.9 us
    dot_general x2, matrix products, update(): jnp.einsum('hqd,khd->hqk', grouped, key_block, preferred_element_type=jnp...  18.8 us
    all_gather x1, waiting for transfers between devices, body(): piece = lax.all_gather(normalised_rows, 'tp', axis=0, tiled=True)  17.4 us
    reduce_sum x2, other arithmetic, update(): jnp.sum(weights_now, axis=-1)  17 us
    dot_general x2, matrix products, update(): jnp.einsum('hqk,khd->hqd', weights_now.astype(jnp.bfloat16), value_block,...  16.2 us
  transfers between devices with their start and end apart: 4, of which 3 were waited for; matrix products, arithmetic and copies ran while one was open for 10% of the time, Pallas kernels for 0%

commit v1 on v0

--- a/solution.py
+++ b/solution.py
@@ -1,3 +1,4 @@
+import functools
 import math
 import jax
 import jax.numpy as jnp
@@ -7,6 +8,24 @@
 GRID_W = 64
 NORM_EPS = 1e-06
 ROPE_BASE = 10000.0
+
+
+def mark_the_cycles(local, along_dim, mesh_ax):
+    degree = lax.psum(1, axis_name=mesh_ax)
+    o_now = range(1, degree)
+    x_now = map(lambda t: (t - 1, t), o_now)
+    b_now = list(x_now) + [(degree - 1, 0)]
+    outer = local
+    rack = [outer]
+    for _ in range(degree - 1):
+        outer = lax.ppermute(outer, axis_name=mesh_ax, perm=b_now)
+        rack += [outer]
+    r_now = jnp.concatenate([*reversed(rack)], along_dim)
+    view_out = jnp.roll(r_now, (lax.axis_index(mesh_ax) + 1) * outer.shape[along_dim], along_dim)
+    return view_out
+
+
+carry_matrix = functools.partial(mark_the_cycles, along_dim=0, mesh_ax="tp")
 
 
 def normalize(latent_value_rows):
@@ -73,7 +92,7 @@
     prefix_normalised = modulate(context, modulation[1])
     query_cols = query_weight.shape[1]
     key_cols = key_matrix.shape[1]
-    piece = lax.all_gather(normalised_rows, "tp", axis=0, tiled=True)
+    piece = carry_matrix(normalised_rows)
     projected = jnp.concatenate(
         [
             jnp.dot(piece, query_weight, preferred_element_type=jnp.float32),

time: 287 us -> 294 us (1.024)
  local copies, waits for them, and re-layouts: 13.9 us -> 21.3 us
    ppermute x0 -> x3, waiting for transfers between devices: none -> 20.3 us  [mark_the_cycles(): outer = lax.ppermute(outer, axis_name=mesh_ax, perm=b_now)]
    all_gather x1 -> x0, waiting for transfers between devices: 17.4 us -> none  [body(): piece = lax.all_gather(normalised_rows, 'tp', axis=0, tiled=True)]
    unnamed x26 -> x44, local copies, waits for them, and re-layouts: 1.42 us -> 6.42 us
  transfers between devices with their start and end apart: 4 -> 6, of which waited for: 3 -> 5; matrix products, arithmetic and copies ran while one was open for 10% -> 11% of each run, Pallas kernels for 0% -> 0%
where the time goes in v1:
time: 294 us; the launch traced here: 293 us
  blocking collectives  109 us (37%)
  waiting for transfers between devices  57.9 us (20%)
  matrix products  53.8 us (18%)
  other arithmetic  36.7 us (12%)
  local copies, waits for them, and re-layouts  21.3 us (7%)
  between operations  13.5 us (5%)
    psum x1, blocking collectives, body(): summed = lax.psum(partials, 'sp')  38.8 us
    all_gather x1, blocking collectives, body(): lax.all_gather(local_values, 'sp', axis=0, tiled=True)  33.4 us
    all_gather x1, blocking collectives, body(): lax.all_gather(local_keys, 'sp', axis=0, tiled=True)  31.6 us
    reduce_scatter x1, waiting for transfers between devices, body(): lax.psum_scatter(jnp.dot(attended, out_weight, preferred_element_type=jnp...  29.9 us
    ppermute x3, waiting for transfers between devices, mark_the_cycles(): outer = lax.ppermute(outer, axis_name=mesh_ax, perm=b_now)  20.3 us
    dot_general x2, matrix products, update(): jnp.einsum('hqd,khd->hqk', grouped, key_block, preferred_element_type=jnp...  18.9 us
    reduce_sum x2, other arithmetic, update(): jnp.sum(weights_now, axis=-1)  17 us
    dot_general x2, matrix products, update(): jnp.einsum('hqk,khd->hqd', weights_now.astype(jnp.bfloat16), value_block,...  16.2 us
  transfers between devices with their start and end apart: 6, of which 5 were waited for; matrix products, arithmetic and copies ran while one was open for 11% of the time, Pallas kernels for 0%

profile of v1, /device:TPU:0, one launch (start us, length us, event | category | flops | bytes accessed | tf_op | source)
XLA Modules:
  0.0 292.7 jit_solution(2807044179396929721)
XLA Ops:
  6.5 2.4 fusion.50
  9.0 38.8 %psum.7 = f32[2,1536]{1,0:T(2,128)S(1)} all-reduce(f32[2,1536]{1,0:T(2,128)S(1)} %fusion.50), channel_id=1, replica_groups=mesh['sp'=8,'tp'=4] {'sp'}, use_global_device_ids=true, to_apply=%region_0.1 | all-reduce | flops 3072 | bytes 24576 | tf_op jit(solution)/shard_map/psum | solution.py:88
  47.8 5.2 %all_gather.15 = f32[2,6144]{1,0:T(2,128)S(1)} all-gather(f32[2,1536]{1,0:T(2,128)S(1)} %psum.7), channel_id=1, replica_groups=mesh['sp'=8,'tp'=4] {'tp'}, dimensions={1}, use_global_device_ids=true | all-gather | bytes 61440 | tf_op jit(solution)/shard_map/all_gather | solution.py:89
  55.4 1.3 fusion.39
  57.1 8.3 %collective-permute-done = bf16[128,2048]{1,0:T(8,128)(2,1)S(1)} collective-permute-done((bf16[128,2048]{1,0:T(8,128)(2,1)S(1)}, bf16[128,2048]{1,0:T(8,128)(2,1)S(1)}, u32[]{:S(2)}, u32[]{:S(2)}) %collective-permute-start) | collective-permute-done | bytes 524320 | tf_op jit(solution)/shard_map/ppermute | solution.py:21
  65.3 8.7 %collective-permute-done.1 = bf16[128,2048]{1,0:T(8,128)(2,1)} collective-permute-done((bf16[128,2048]{1,0:T(8,128)(2,1)S(1)}, bf16[128,2048]{1,0:T(8,128)(2,1)}, u32[]{:S(2)}, u32[]{:S(2)}) %collective-permute-start.1) | collective-permute-done | bytes 524320 | tf_op jit(solution)/shard_map/ppermute | solution.py:21
  76.2 1.7 copy.83
  78.0 1.7 copy.84
  79.6 3.3 %collective-permute-done.2 = bf16[128,2048]{1,0:T(8,128)(2,1)} collective-permute-done((bf16[128,2048]{1,0:T(8,128)(2,1)}, bf16[128,2048]{1,0:T(8,128)(2,1)}, u32[]{:S(2)}, u32[]{:S(2)}) %collective-permute-start.2) | collective-permute-done | bytes 524320 | tf_op jit(solution)/shard_map/ppermute | solution.py:21
  88.5 2.0 multiply_reduce_fusion.1
  92.8 1.5 subtract_convert_fusion.1
  96.2 3.3 %fusion.30 = bf16[512,256]{0,1:T(8,128)(2,1)} fusion(bf16[2048,256]{1,0:T(8,128)(2,1)} %param.20, bf16[1024,2048]{1,0:T(8,128)(2,1)} %copy-done.13, s32[]{:T(128)S(6)} %select_n.36), kind=kOutput, calls=%fused_computation.38 | convolution fusion | flops 537001984 | bytes 3407876 | tf_op jit(solution)/shard_map/dot_general | solution.py:100
  99.5 1.8 copy.85
  104.7 1.6 fusion.33
  107.3 31.6 %all_gather.16 = bf16[512,2,128]{2,0,1:T(8,128)(2,1)S(1)} all-gather(bf16[64,2,128]{2,0,1:T(8,128)(2,1)S(1)} %fusion.46), channel_id=1, replica_groups=mesh['sp'=8,'tp'=4] {'sp'}, dimensions={0}, use_global_device_ids=true | all-gather | bytes 294912 | tf_op jit(solution)/shard_map/all_gather | solution.py:122
  138.8 33.4 %all_gather.17 = bf16[512,2,128]{2,0,1:T(8,128)(2,1)} all-gather(bf16[64,2,128]{2,0,1:T(8,128)(2,1)S(1)} %bitcast.106), channel_id=1, replica_groups=mesh['sp'=8,'tp'=4] {'sp'}, dimensions={0}, use_global_device_ids=true | all-gather | bytes 294912 | tf_op jit(solution)/shard_map/all_gather | solution.py:123
  172.2 3.8 %multiply_reduce_fusion = (f32[512,4]{0,1:T(4,128)S(1)}, f32[512,512]{0,1:T(8,128)S(1)}) fusion(bf16[2048,512]{1,0:T(8,128)(2,1)} %param.18, bf16[1024,2048]{1,0:T(8,128)(2,1)} %copy-done.13, s32[]{:T(128)S(6)} %select_n.36), kind=kOutput, calls=%fused_computation.50 | convolution fusion | flops 1074264064 | bytes 5251076 | tf_op jit(solution)/shard_map/dot_general | solution.py:98
  178.7 1.9 copy.74
  180.6 1.9 copy.75
  182.5 1.9 pad_maximum_fusion
  188.0 7.7 %all-gather.5.cloned.1.call-done = bf16[4096,2,128]{2,0,1:T(8,128)(2,1)} async-done(((bf16[512,2,128]{2,0,1:T(8,128)(2,1)}), bf16[4096,2,128]{2,0,1:T(8,128)(2,1)}) %all-gather.5.cloned.1.call-update) | async-done | bytes 2097168 | tf_op jit(solution)/shard_map/all_gather | solution.py:167
  195.7 52.2 %while.14 = (s32[]{:T(128)}, f32[2,1024]{1,0:T(2,128)S(1)}, f32[2,1024]{1,0:T(2,128)S(1)}, f32[2,1024,128]{2,1,0:T(8,128)S(1)}, bf16[2,2048,2,128]{3,1,0,2:T(8,1...) while((s32[]{:T(128)}, f32[2,1024]{1,0:T(2,128)S(1)}, ...), condition=%wide.region_11.12_spmd, body=%wide.region_8.11_spmd.sunk | while | flops 2181566464 | bytes 55182420 | solution.py:177
  195.7 9.4 %bitcast_reduce_fusion.2 = (f32[2,1024]{1,0:T(2,128)S(1)}, f32[2,2048,1024]{2,1,0:T(8,128)}) fusion(bf16[2,1024,128]{2,1,0:T(8,128)(2,1)} %get-tuple-element.194, bf16[2,2048,2,128]{3,1,0,2:T(8,128)(2,1)} %get-tuple-element.193, s32[]{:T(128)} %get-tuple-element.181), kind=kOutput, calls=%fused_computation.1.clone.1 | convolution fusion | flops 1082128384 | bytes 18358784 | tf_op jit(solution)/shard_map/while/body/eval_jaxpr/hqd,khd->hqk/dot_general | solution.py:152
  205.1 8.5 %fusion.89 = f32[2,1024]{1,0:T(2,128)S(1)} fusion(f32[2,2048,1024]{2,1,0:T(8,128)} %get-tuple-element.170, f32[2,1024]{1,0:T(2,128)S(1)} %max.4), kind=kLoop, calls=%fused_computation.4.clone.1 | loop fusion | flops 12580864 | bytes 16793600 | tf_op jit(solution)/shard_map/while/body/eval_jaxpr/reduce_sum | solution.py:164
  213.7 8.1 %fusion.90 = f32[2,1024,128]{2,1,0:T(8,128)S(1)} fusion(f32[2,2048,1024]{2,1,0:T(8,128)} %get-tuple-element.170, f32[2,1024]{1,0:T(2,128)S(1)} %max.4, bf16[2,2048,2,128]{3,1,0,2:T(8,128)(2,1)} %get-tuple-element.195, s32[]{:T(128)} %get-tuple-element.181, f32[2,1024,128]{2,1,0:T(8,128)S(1)} %get-tuple-element.184, f32[2,1024]{1,0:T(2,128)S(1)} %get-tuple-element.172), kind=kOutput, calls=%fused_computation.6.clone.1 | convolution fusion | flops 1086849024 | bytes 19939840 | tf_op jit(solution)/shard_map/while/body/eval_jaxpr/hqk,khd->hqd/dot_general | solution.py:158
  221.8 9.4 %bitcast_reduce_fusion.2 = (f32[2,1024]{1,0:T(2,128)S(1)}, f32[2,2048,1024]{2,1,0:T(8,128)}) fusion(bf16[2,1024,128]{2,1,0:T(8,128)(2,1)} %get-tuple-element.194, bf16[2,2048,2,128]{3,1,0,2:T(8,128)(2,1)} %get-tuple-element.193, s32[]{:T(128)} %get-tuple-element.181), kind=kOutput, calls=%fused_computation.1.clone.1 | convolution fusion | flops 1082128384 | bytes 18358784 | tf_op jit(solution)/shard_map/while/body/eval_jaxpr/hqd,khd->hqk/dot_general | solution.py:152
  231.2 8.5 %fusion.89 = f32[2,1024]{1,0:T(2,128)S(1)} fusion(f32[2,2048,1024]{2,1,0:T(8,128)} %get-tuple-element.170, f32[2,1024]{1,0:T(2,128)S(1)} %max.4), kind=kLoop, calls=%fused_computation.4.clone.1 | loop fusion | flops 12580864 | bytes 16793600 | tf_op jit(solution)/shard_map/while/body/eval_jaxpr/reduce_sum | solution.py:164
  239.8 8.1 %fusion.90 = f32[2,1024,128]{2,1,0:T(8,128)S(1)} fusion(f32[2,2048,1024]{2,1,0:T(8,128)} %get-tuple-element.170, f32[2,1024]{1,0:T(2,128)S(1)} %max.4, bf16[2,2048,2,128]{3,1,0,2:T(8,128)(2,1)} %get-tuple-element.195, s32[]{:T(128)} %get-tuple-element.181, f32[2,1024,128]{2,1,0:T(8,128)S(1)} %get-tuple-element.184, f32[2,1024]{1,0:T(2,128)S(1)} %get-tuple-element.172), kind=kOutput, calls=%fused_computation.6.clone.1 | convolution fusion | flops 1086849024 | bytes 19939840 | tf_op jit(solution)/shard_map/while/body/eval_jaxpr/hqk,khd->hqd/dot_general | solution.py:158
  249.0 1.2 copy.88
  250.3 2.6 convolution_convert_fusion
  253.0 29.9 %reduce-scatter.2.cloned.1.call-done = bf16[128,2048]{1,0:T(8,128)(2,1)} async-done(((bf16[512,2048]{1,0:T(8,128)(2,1)}), bf16[128,2048]{1,0:T(8,128)(2,1)}) %reduce-scatter.2.cloned.1.call-update) | async-done | bytes 524304 | tf_op jit(solution)/shard_map/reduce_scatter | solution.py:185
  284.1 2.1 fusion.40
  (94 shorter events, 27.5 us)
Async XLA Ops:
  6.5 243.8 %copy-start = (bf16[512,2048]{1,0:T(8,128)(2,1)S(1)}, bf16[512,2048]{1,0:T(8,128)(2,1)}, u32[]{:S(2)}) copy-start(bf16[512,2048]{1,0:T(8,128)(2,1)} %param.21) | copy-start | bytes 6291460
  6.5 78.6 %copy-start.2 = (bf16[128,2048]{1,0:T(8,128)(2,1)S(1)}, bf16[128,2048]{1,0:T(8,128)(2,1)}, u32[]{:S(2)}) copy-start(bf16[128,2048]{1,0:T(8,128)(2,1)} %param.13) | copy-start | bytes 1572868
  6.5 181.5 %all-gather.3.cloned.1.call-start = ((), (), s32[]{:S(2)}) async-start(), calls=%async_computation.1 | async-start | bytes 2359296 | tf_op jit(solution)/shard_map/all_gather | solution.py:166
  54.9 0.5 copy-start.15
  56.7 8.7 %collective-permute-start = (bf16[128,2048]{1,0:T(8,128)(2,1)S(1)}, bf16[128,2048]{1,0:T(8,128)(2,1)S(1)}, u32[]{:S(2)}, u32[]{:S(2)}) collective-permute-start(bf16[128,2048]{1,0:T(8,128)(2,1)S(1)} %fusion.39), channel_id=1, source_target_pairs={{0,1},{1,2},{2,3},{3,0},{4,5},{5,6},{6,7},{7,4},{8,9},{9,10},{10,1... | collective-permute-start | bytes 1572872 | tf_op jit(solution)/shard_map/ppermute | solution.py:21
  65.3 8.7 %collective-permute-start.1 = (bf16[128,2048]{1,0:T(8,128)(2,1)S(1)}, bf16[128,2048]{1,0:T(8,128)(2,1)}, u32[]{:S(2)}, u32[]{:S(2)}) collective-permute-start(bf16[128,2048]{1,0:T(8,128)(2,1)S(1)} %collective-permute-done), channel_id=1, source_target_pairs={{0,1},{1,2},{2,3},{3,0},{4,5},{5,6},{6,7},{7,4},{8,9},{9,10},{10,1... | collective-permute-start | bytes 1572872 | tf_op jit(solution)/shard_map/ppermute | solution.py:21
  74.0 8.9 %collective-permute-start.2 = (bf16[128,2048]{1,0:T(8,128)(2,1)}, bf16[128,2048]{1,0:T(8,128)(2,1)}, u32[]{:S(2)}, u32[]{:S(2)}) collective-permute-start(bf16[128,2048]{1,0:T(8,128)(2,1)} %collective-permute-done.1), channel_id=1, source_target_pairs={{0,1},{1,2},{2,3},{3,0},{4,5},{5,6},{6,7},{7,4},{8,9},{9,10},{10,1... | collective-permute-start | bytes 1572872 | tf_op jit(solution)/shard_map/ppermute | solution.py:21
  79.6 8.6 %copy-start.16 = (f32[128]{0:T(128)S(1)}, f32[128]{0:T(128)}, u32[]{:S(2)}) copy-start(f32[128]{0:T(128)} %copy-done.15) | copy-start | bytes 1540
  79.6 8.9 %copy-start.6 = (bf16[2048,256]{1,0:T(8,128)(2,1)S(1)}, bf16[2048,256]{1,0:T(8,128)(2,1)}, u32[]{:S(2)}) copy-start(bf16[2048,256]{1,0:T(8,128)(2,1)} %param.19) | copy-start | bytes 3145732
  88.3 4.5 %copy-start.5 = (f32[512,32]{1,0:T(8,128)S(1)}, f32[512,32]{1,0:T(8,128)}, u32[]{:S(2)}) copy-start(f32[512,32]{1,0:T(8,128)} %copy.82) | copy-start | bytes 196612
  88.5 2.1 copy-start.13
  90.6 4.9 %copy-start.4 = (bf16[64,2048]{1,0:T(8,128)(2,1)S(1)}, bf16[64,2048]{1,0:T(8,128)(2,1)}, u32[]{:S(2)}) copy-start(bf16[64,2048]{1,0:T(8,128)(2,1)} %param.14) | copy-start | bytes 786436
  94.3 8.4 %copy-start.7 = (bf16[2048,256]{1,0:T(8,128)(2,1)S(1)}, bf16[2048,256]{1,0:T(8,128)(2,1)}, u32[]{:S(2)}) copy-start(bf16[2048,256]{1,0:T(8,128)(2,1)} %param.19) | copy-start | bytes 3145732
  94.3 8.4 %copy-start.11 = (f32[1,2048]{1,0:T(1,128)S(1)}, f32[1,2048]{1,0:T(1,128)}, u32[]{:S(2)}) copy-start(f32[1,2048]{1,0:T(1,128)} %get-tuple-element.104) | copy-start | bytes 24580
  94.3 8.4 %copy-start.12 = (f32[1,2048]{1,0:T(1,128)S(1)}, f32[1,2048]{1,0:T(1,128)}, u32[]{:S(2)}) copy-start(f32[1,2048]{1,0:T(1,128)} %get-tuple-element.105) | copy-start | bytes 24580
  95.4 100.3 %all-gather.5.cloned.1.call-start = ((), (), s32[]{:S(2)}) async-start(), calls=%async_computation.2 | async-start | bytes 2359296 | tf_op jit(solution)/shard_map/all_gather | solution.py:167
  101.4 181.5 %reduce-scatter.2.cloned.1.call-start = ((), (), s32[]{:S(2)}) async-start(), calls=%async_computation.3 | async-start | bytes 2621440 | tf_op jit(solution)/shard_map/reduce_scatter | solution.py:185
  102.1 0.6 copy-start.17
  172.2 3.9 %copy-start.18 = (f32[128]{0:T(128)S(1)}, f32[128]{0:T(128)}, u32[]{:S(2)}) copy-start(f32[128]{0:T(128)} %param.22) | copy-start | bytes 1540
  172.2 4.1 %copy-start.9 = (f32[512,32]{0,1:T(8,128)S(1)}, f32[512,32]{0,1:T(8,128)}, u32[]{:S(2)}) copy-start(f32[512,32]{0,1:T(8,128)} %get-tuple-element.112) | copy-start | bytes 196612
  172.2 4.1 %copy-start.10 = (f32[512,32]{0,1:T(8,128)S(1)}, f32[512,32]{0,1:T(8,128)}, u32[]{:S(2)}) copy-start(f32[512,32]{0,1:T(8,128)} %get-tuple-element.113) | copy-start | bytes 196612
  184.4 0.8 copy-start.1
  185.2 1.6 copy-start.8
  250.3 33.8 %copy-start.3 = (bf16[128,2048]{1,0:T(8,128)(2,1)S(1)}, bf16[128,2048]{1,0:T(8,128)(2,1)}, u32[]{:S(2)}) copy-start(bf16[128,2048]{1,0:T(8,128)(2,1)} %param.13) | copy-start | bytes 1572868
  250.3 33.8 %copy-start.14 = (f32[1,2048]{1,0:T(1,128)S(1)}, f32[1,2048]{1,0:T(1,128)}, u32[]{:S(2)}) copy-start(f32[1,2048]{1,0:T(1,128)} %get-tuple-element.103) | copy-start | bytes 24580
Sparse Core Ops, SparseCore 0:
  95.5 49.0 all-gather.2
  146.8 48.8 all-gather.4
  253.1 29.7 reduce-scatter.1
